TPU v7x, 32 devices: a whole 2x2x4 slice. The times are simulated.
32 devices in a mesh: kv: 8 (over z, y), tp: 4 (over x, core).
Axes of the slice: x: 2, y: 2, z: 4, core: 2. Of those that a mesh axis runs over, the one named last changes fastest.
Arguments:
- hidden_in: bfloat16 [16, 4096], P(None, ('kv', 'tp')), may hold values from -12 to 12
- attn_gain: float32 [4096], P('kv'), may hold values from 0.1 to 1.9
- query_weight: bfloat16 [4096, 4096], P('kv', 'tp'), may hold values from -0.09375 to 0.09375
- key_cache: bfloat16 [16, 8192, 8, 128], P(None, 'kv', 'tp'), may hold values from -600 to 600
- value_cache: bfloat16 [16, 8192, 8, 128], P(None, 'kv', 'tp'), may hold values from -6 to 6
- lambdas: float32 [32], P('tp'), may hold values from 0.3 to 0.8
- head_gain: float32 [128], replicated, may hold values from 0.1 to 1.9
- out_weight: bfloat16 [4096, 4096], P('tp', 'kv'), may hold values from -0.09375 to 0.09375
- mixer_gain: float32 [4096], P(('kv', 'tp')), may hold values from 0.1 to 1.9
- gate_weight: bfloat16 [4096, 11264], P('kv', 'tp'), may hold values from -0.09375 to 0.09375
- up_weight: bfloat16 [4096, 11264], P('kv', 'tp'), may hold values from -0.09375 to 0.09375
- down_weight: bfloat16 [11264, 4096], P('tp', 'kv'), may hold values from -0.0546875 to 0.0546875
Outputs:
- mixed: bfloat16 [16, 4096], P(None, ('kv', 'tp'))
All inputs are finite; a program needn't handle non-finite values.
Results may differ from a plain program's by a relative error of at most 0.017.
Values may be sent and summed in bfloat16 or wider, within the bound.
A program may use at most 64 MiB of HBM per device.

v0:
```python
import jax
import jax.numpy as jnp
from jax import lax
from jax.sharding import PartitionSpec as P

D = 4096
HEAD_DIM = 64
eps = 1e-06


def finish_heads(totals, weighted, lambdas, head_gain, kv_dev, group_size):
    head_means = weighted / totals[..., None]
    mixing = lambdas.reshape(kv_dev, group_size)
    attended = head_means[0] - mixing[None, :, :, None] * head_means[1]
    norm_inv = lax.rsqrt(jnp.mean(attended * attended, axis=-1, keepdims=True) + eps)
    head_out = (attended * norm_inv * head_gain).astype(jnp.bfloat16)
    return head_out.reshape(head_out.shape[0], kv_dev * group_size * 2 * HEAD_DIM)


def per_device(
    hidden_in,
    attn_gain,
    query_weight,
    key_cache,
    value_cache,
    lambdas,
    head_gain,
    out_weight,
    mixer_gain,
    gate_weight,
    up_weight,
    down_weight,
):
    batch_rows = hidden_in.shape[0]
    rows_block = lax.all_gather(hidden_in, "tp", axis=1, tiled=True)
    block_f = rows_block.astype(jnp.float32)
    gained = (block_f * attn_gain).astype(jnp.bfloat16)
    partial_value = jnp.dot(gained, query_weight, preferred_element_type=jnp.float32)
    own_cols = hidden_in.astype(jnp.float32)
    squares = lax.psum(jnp.sum(own_cols * own_cols, axis=1), ("kv", "tp"))
    query_full = lax.psum(partial_value, "kv")
    row_scale = lax.rsqrt(squares / D + eps)
    query_rows = (query_full * row_scale[:, None]).astype(jnp.bfloat16)
    positions = key_cache.shape[1]
    kv_dev = key_cache.shape[2]
    heads_dev = query_rows.shape[1] // (2 * HEAD_DIM)
    group_size = heads_dev // kv_dev
    query_heads = query_rows.reshape(batch_rows, kv_dev, group_size, 2, HEAD_DIM)
    key_rows = key_cache.reshape(batch_rows, positions, kv_dev, 2, HEAD_DIM)
    scores = jnp.einsum(
        "bkgcd,bpkcd->cbkgp", query_heads, key_rows, preferred_element_type=jnp.float32
    ) * HEAD_DIM ** (-0.5)
    maxima = jnp.max(scores, axis=-1)
    exponent = jnp.exp(scores - maxima[..., None])
    totals = jnp.sum(exponent, axis=-1)
    exp_weights = exponent.astype(jnp.bfloat16)
    weighted = jnp.einsum(
        "cbkgp,bpkv->cbkgv", exp_weights, value_cache, preferred_element_type=jnp.float32
    )
    parts_max, parts_tot, parts_acc = (
        lax.all_to_all(maxima[None], "kv", split_axis=2, concat_axis=0, tiled=True),
        lax.all_to_all(totals[None], "kv", split_axis=2, concat_axis=0, tiled=True),
        lax.all_to_all(weighted[None], "kv", split_axis=2, concat_axis=0, tiled=True),
    )
    top = jnp.max(parts_max, axis=0)
    factors = jnp.exp(parts_max - top[None])
    own_tot = jnp.sum(parts_tot * factors, axis=0)
    own_acc = jnp.sum(parts_acc * factors[..., None], axis=0)
    own_out = finish_heads(own_tot, own_acc, lambdas, head_gain, kv_dev, group_size)
    head_out = lax.all_gather(own_out, "kv", axis=0, tiled=True)
    projected = jnp.dot(head_out, out_weight, preferred_element_type=jnp.float32)
    attn_out = lax.psum_scatter(
        projected.astype(jnp.bfloat16), "tp", scatter_dimension=1, tiled=True
    ).astype(jnp.float32)
    after_attn = (hidden_in.astype(jnp.float32) + attn_out).astype(jnp.bfloat16)
    after_f = after_attn.astype(jnp.float32)
    squares_two = lax.psum(jnp.sum(after_f * after_f, axis=1), ("kv", "tp"))
    mixer_in = (after_f * lax.rsqrt(squares_two / D + eps)[:, None] * mixer_gain).astype(
        jnp.bfloat16
    )
    gathered = lax.all_gather(mixer_in, "tp", axis=1, tiled=True)
    gate_part = jnp.dot(gathered, gate_weight, preferred_element_type=jnp.float32)
    up_part = jnp.dot(gathered, up_weight, preferred_element_type=jnp.float32)
    gate_sum, up_sum = lax.psum((gate_part, up_part), "kv")
    hidden = (jax.nn.silu(gate_sum) * up_sum).astype(jnp.bfloat16)
    down_part = jnp.dot(hidden, down_weight, preferred_element_type=jnp.float32)
    mixer_out = lax.psum_scatter(
        down_part.astype(jnp.bfloat16), "tp", scatter_dimension=1, tiled=True
    ).astype(jnp.float32)
    return (after_f + mixer_out).astype(jnp.bfloat16)


def solution(mesh):
    in_specs = (
        P(None, ("kv", "tp")),
        P("kv"),
        P("kv", "tp"),
        P(None, "kv", "tp", None),
        P(None, "kv", "tp", None),
        P("tp"),
        P(),
        P("tp", "kv"),
        P(("kv", "tp")),
        P("kv", "tp"),
        P("kv", "tp"),
        P("tp", "kv"),
    )
    out_specs = P(None, ("kv", "tp"))
    return jax.shard_map(
        per_device, mesh=mesh, in_specs=in_specs, out_specs=out_specs, check_vma=False
    )
```

profile of v0, /device:TPU:0, one launch (start us, length us, event | category | flops | bytes accessed | tf_op | source)
XLA Modules:
  0.0 329.5 jit_solution(1171620726180046008)
XLA Ops:
  6.5 6.5 %all_gather.9 = bf16[16,512]{1,0:T(8,128)(2,1)S(1)} all-gather(bf16[16,128]{1,0:T(8,128)(2,1)} %param.12), channel_id=1, replica_groups=mesh['kv'=8,'tp'=4] {'tp'}, dimensions={1}, use_global_device_ids=true | all-gather | bytes 20480 | tf_op jit(solution)/shard_map/all_gather | solution.py:35
  13.8 2.1 fusion.15
  16.0 41.0 %psum.36 = f32[16]{0:T(128)S(1)} all-reduce(f32[16]{0:T(128)S(1)} %fusion.17), channel_id=1, replica_groups=mesh['kv'=8,'tp'=4] {'kv','tp'}, use_global_device_ids=true, to_apply=%region_2.0 | all-reduce | flops 16 | bytes 128 | tf_op jit(solution)/shard_map/psum | solution.py:40
  57.0 21.2 %copy.33 = bf16[16,1024,2,128]{1,3,2,0:T(8,128)(2,1)} copy(bf16[16,1024,2,128]{3,2,1,0:T(2,128)(2,1)} %param.15) | data formatting | bytes 16777216 | tf_op args[3]
  78.2 9.0 %all-reduce.4.cloned.1.call-done = f32[16,1024]{1,0:T(8,128)} async-done(((f32[16,1024]{1,0:T(8,128)}), f32[16,1024]{1,0:T(8,128)}) %all-reduce.4.cloned.1.call-update) | async-done | bytes 65552 | tf_op jit(solution)/shard_map/psum | solution.py:41
  87.1 0.9 multiply_convert_fusion.2
  88.2 4.7 %fusion.28 = (f32[2,16,2,4]{3,2,1,0:T(2,128)S(1)}, f32[2,16,2,4,1024]{4,3,2,1,0:T(4,128)S(1)}) fusion(bf16[16,1024,2,2,64]{1,4,3,2,0:T(8,128)(2,1)} %bitcast.56, bf16[16,2,4,2,64]{4,3,2,1,0:T(2,128)(2,1)S(1)} %reshape.35), kind=kOutput, calls=%fused_computation.46 | convolution fusion | flops 34078464 | bytes 9470976 | tf_op jit(solution)/shard_map/bkgcd,bpkcd->cbkgp/dot_general | solution.py:50
  94.1 4.5 %all-to-all-start.2 = ((f32[1,2,16,2,4]{4,3,1,0,2:T(2,128)}), f32[1,2,16,2,4]{4,3,1,0,2:T(2,128)S(1)}, u32[]{:S(2)}, u32[]{:S(2)}) async-start(f32[1,2,16,2,4]{4,3,1,0,2:T(2,128)} %copy.41), calls=%async_computation.2 | async-start | bytes 65536 | tf_op jit(solution)/shard_map/all_to_all | solution.py:62
  99.3 6.1 %all-to-all-done.2 = f32[1,2,16,2,4]{4,3,1,0,2:T(2,128)S(1)} async-done(((f32[1,2,16,2,4]{4,3,1,0,2:T(2,128)}), f32[1,2,16,2,4]{4,3,1,0,2:T(2,128)S(1)}, u32[]{:S(2)}, u32[]{:S(2)}) %all-to-all-start.2) | async-done | bytes 1056 | tf_op jit(solution)/shard_map/all_to_all | solution.py:62
  105.3 3.3 %all-to-all-start.1 = ((f32[1,2,16,2,4]{4,3,1,0,2:T(2,128)}), f32[1,2,16,2,4]{4,3,1,0,2:T(2,128)S(1)}, u32[]{:S(2)}, u32[]{:S(2)}) async-start(f32[1,2,16,2,4]{4,3,1,0,2:T(2,128)} %copy.39), calls=%async_computation.1 | async-start | bytes 65536 | tf_op jit(solution)/shard_map/all_to_all | solution.py:61
  108.7 5.5 %fusion.7 = f32[1,2,16,2,4,128]{5,4,1,3,0,2:T(4,128)} fusion(bf16[16,1024,2,128,1]{3,2,1,0,4:T(2,128)(2,1)} %bitcast.69, bf16[2,16,2,4,1024]{4,3,2,1,0:T(4,128)(2,1)S(1)} %get-tuple-element.10), kind=kOutput, calls=%fused_computation.5 | convolution fusion | flops 67108864 | bytes 9043968 | tf_op jit(solution)/shard_map/cbkgp,bpkv->cbkgv/dot_general | solution.py:57
  114.2 1.1 all-to-all-done.1
  115.3 4.8 %all-to-all-start = ((f32[1,2,16,2,4,128]{5,4,1,3,0,2:T(4,128)}), f32[1,2,16,2,4,128]{5,4,1,3,0,2:T(4,128)S(1)}, u32[]{:S(2)}, u32[]{:S(2)}) async-start(f32[1,2,16,2,4,128]{5,4,1,3,0,2:T(4,128)} %fusion.7), calls=%async_computation | async-start | bytes 262144 | tf_op jit(solution)/shard_map/all_to_all | solution.py:63
  120.4 7.1 %all-to-all-done = f32[1,2,16,2,4,128]{5,4,1,3,0,2:T(4,128)S(1)} async-done(((f32[1,2,16,2,4,128]{5,4,1,3,0,2:T(4,128)}), f32[1,2,16,2,4,128]{5,4,1,3,0,2:T(4,128)S(1)}, u32[]{:S(2)}, u32[]{:S(2)}) %all-to-all-start) | async-done | bytes 131104 | tf_op jit(solution)/shard_map/all_to_all | solution.py:63
  128.1 30.6 %all-gather = bf16[8,2,1024]{2,1,0:T(2,128)(2,1)S(1)} all-gather(bf16[1,2,1024]{2,1,0:T(2,128)(2,1)S(1)} %fusion.25), channel_id=1, replica_groups=mesh['kv'=8,'tp'=4] {'kv'}, dimensions={0}, use_global_device_ids=true | all-gather | bytes 36864 | tf_op jit(solution)/shard_map/all_gather | solution.py:70
  158.8 1.5 convolution_convert_fusion.1
  161.1 17.5 %reduce-scatter.7.cloned.1.call-done = bf16[128,16]{1,0:T(8,128)(2,1)} async-done(((bf16[512,16]{1,0:T(8,128)(2,1)}), bf16[128,16]{1,0:T(8,128)(2,1)}) %reduce-scatter.7.cloned.1.call-update) | async-done | bytes 4112
  179.5 39.3 %psum.37 = f32[16]{0:T(128)S(1)} all-reduce(f32[16]{0:T(128)S(1)} %fusion.19), channel_id=1, replica_groups=mesh['kv'=8,'tp'=4] {'kv','tp'}, use_global_device_ids=true, to_apply=%region_11.0 | all-reduce | flops 16 | bytes 128 | tf_op jit(solution)/shard_map/psum | solution.py:77
  218.9 5.6 %all_gather.11 = bf16[16,512]{1,0:T(8,128)(2,1)S(1)} all-gather(bf16[16,128]{1,0:T(8,128)(2,1)S(1)} %fusion.21), channel_id=1, replica_groups=mesh['kv'=8,'tp'=4] {'tp'}, dimensions={1}, use_global_device_ids=true | all-gather | bytes 20480 | tf_op jit(solution)/shard_map/all_gather | solution.py:81
  224.5 1.2 fusion.29
  225.6 1.2 fusion.30
  226.9 72.3 %all-reduce.6.cloned.1.call-done = (f32[16,2816]{1,0:T(8,128)}, f32[16,2816]{1,0:T(8,128)}) async-done(((f32[16,2816]{1,0:T(8,128)}, f32[16,2816]{1,0:T(8,128)}), (f32[16,2816]{1,0:T(8,128)}, f32[16,2816]{1,0:T(8,128)})) %all-reduce.6.cloned.1.call-update) | async-done | bytes 360464 | tf_op jit(solution)/shard_map/psum | solution.py:84
  299.2 2.5 convolution_convert_fusion
  302.5 19.1 %reduce-scatter.9.cloned.1.call-done = bf16[128,16]{1,0:T(8,128)(2,1)} async-done(((bf16[512,16]{1,0:T(8,128)(2,1)}), bf16[128,16]{1,0:T(8,128)(2,1)}) %reduce-scatter.9.cloned.1.call-update) | async-done | bytes 4112
  (52 shorter events, 7.8 us)
Async XLA Ops:
  6.5 217.9 %copy-start = (bf16[512,2816]{1,0:T(8,128)(2,1)S(1)}, bf16[512,2816]{1,0:T(8,128)(2,1)}, u32[]{:S(2)}) copy-start(bf16[512,2816]{1,0:T(8,128)(2,1)} %param.21) | copy-start | bytes 8650756
  6.5 80.6 %all-reduce.4.cloned.1.call-start = ((), (), s32[]{:S(2)}) async-start(), calls=%async_computation.5 | async-start | bytes 131072 | tf_op jit(solution)/shard_map/psum | solution.py:41
  94.1 11.2 %all-to-all-start.2 = ((f32[1,2,16,2,4]{4,3,1,0,2:T(2,128)}), f32[1,2,16,2,4]{4,3,1,0,2:T(2,128)S(1)}, u32[]{:S(2)}, u32[]{:S(2)}) async-start(f32[1,2,16,2,4]{4,3,1,0,2:T(2,128)} %copy.41), calls=%async_computation.2 | async-start | bytes 65536 | tf_op jit(solution)/shard_map/all_to_all | solution.py:62
  105.3 10.0 %all-to-all-start.1 = ((f32[1,2,16,2,4]{4,3,1,0,2:T(2,128)}), f32[1,2,16,2,4]{4,3,1,0,2:T(2,128)S(1)}, u32[]{:S(2)}, u32[]{:S(2)}) async-start(f32[1,2,16,2,4]{4,3,1,0,2:T(2,128)} %copy.39), calls=%async_computation.1 | async-start | bytes 65536 | tf_op jit(solution)/shard_map/all_to_all | solution.py:61
  108.7 11.5 %copy-start.5 = (f32[8]{0:T(128)S(1)}, f32[8]{0:T(128)}, u32[]{:S(2)}) copy-start(f32[8]{0:T(128)} %param.17) | copy-start | bytes 100
  108.7 19.4 %copy-start.3 = (f32[128]{0:T(128)S(1)}, f32[128]{0:T(128)}, u32[]{:S(2)}) copy-start(f32[128]{0:T(128)} %param.18) | copy-start | bytes 1540
  108.7 70.7 %copy-start.2 = (bf16[16,128]{1,0:T(8,128)(2,1)S(1)}, bf16[16,128]{1,0:T(8,128)(2,1)}, u32[]{:S(2)}) copy-start(bf16[16,128]{1,0:T(8,128)(2,1)} %param.12) | copy-start | bytes 12292
  108.7 110.1 %copy-start.4 = (f32[128]{0:T(128)S(1)}, f32[128]{0:T(128)}, u32[]{:S(2)}) copy-start(f32[128]{0:T(128)} %param.20) | copy-start | bytes 1540
  115.3 12.2 %all-to-all-start = ((f32[1,2,16,2,4,128]{5,4,1,3,0,2:T(4,128)}), f32[1,2,16,2,4,128]{5,4,1,3,0,2:T(4,128)S(1)}, u32[]{:S(2)}, u32[]{:S(2)}) async-start(f32[1,2,16,2,4,128]{5,4,1,3,0,2:T(4,128)} %fusion.7), calls=%async_computation | async-start | bytes 262144 | tf_op jit(solution)/shard_map/all_to_all | solution.py:63
  120.1 58.4 %reduce-scatter.7.cloned.1.call-start = ((), (), s32[]{:S(2)}) async-start(), calls=%async_computation.6 | async-start | bytes 163840
  161.0 138.2 %all-reduce.6.cloned.1.call-start = ((), (), s32[]{:S(2)}) async-start(), calls=%async_computation.8 | async-start | bytes 720896 | tf_op jit(solution)/shard_map/psum | solution.py:84
  218.8 6.8 %copy-start.1 = (bf16[512,2816]{1,0:T(8,128)(2,1)S(1)}, bf16[512,2816]{1,0:T(8,128)(2,1)}, u32[]{:S(2)}) copy-start(bf16[512,2816]{1,0:T(8,128)(2,1)} %param.22) | copy-start | bytes 8650756
  226.8 94.8 %reduce-scatter.9.cloned.1.call-start = ((), (), s32[]{:S(2)}) async-start(), calls=%async_computation.7 | async-start | bytes 163840
Sparse Core Ops, SparseCore 0:
  16.1 71.0 all-reduce.3
  161.1 17.3 reduce-scatter.6
  226.9 72.2 all-reduce.5
  302.6 18.9 reduce-scatter.8
where the time goes:
time: 331 us; the launch traced here: 330 us
  waiting for transfers between devices  132 us (40%)
  blocking collectives  123 us (37%)
  local copies, waits for them, and re-layouts  26 us (8%)
  matrix products  18.6 us (6%)
  between operations  13.3 us (4%)
  starting transfers between devices  12.8 us (4%)
  other arithmetic  3.66 us (1%)
    psum x1, waiting for transfers between devices, per_device(): gate_sum, up_sum = lax.psum((gate_part, up_part), 'kv')  72.3 us
    psum x1, blocking collectives, per_device(): squares = lax.psum(jnp.sum(own_cols * own_cols, axis=1), ('kv', 'tp'))  41 us
    psum x1, blocking collectives, per_device(): squares_two = lax.psum(jnp.sum(after_f * after_f, axis=1), ('kv', 'tp'))  39.3 us
    unnamed x6, waiting for transfers between devices  36.7 us
    all_gather x1, blocking collectives, per_device(): head_out = lax.all_gather(own_out, 'kv', axis=0, tiled=True)  30.6 us
    unnamed x18, local copies, waits for them, and re-layouts  24.3 us
    psum x1, waiting for transfers between devices, per_device(): query_full = lax.psum(partial_value, 'kv')  8.99 us
    all_to_all x1, waiting for transfers between devices, per_device(): lax.all_to_all(weighted[None], 'kv', split_axis=2, concat_axis=0, tiled=T...  7.09 us
  transfers between devices with their start and end apart: 7, of which 7 were waited for; matrix products, arithmetic and copies ran while one was open for 8% of the time, Pallas kernels for 0%

commit v1 on v0

--- a/solution.py
+++ b/solution.py
@@ -6,6 +6,17 @@
 D = 4096
 HEAD_DIM = 64
 eps = 1e-06
+
+
+def turned_line(x, axis, d):
+    size = lax.axis_size(axis)
+    forward = [(i, (i + 1) % size) for i in range(size)]
+    parts = [x]
+    for hop in range(1, size):
+        parts = [lax.ppermute(parts[0], axis, forward), *parts]
+    whole = jnp.concatenate(parts, axis=d)
+    shift = (lax.axis_index(axis) + 1) * parts[-1].shape[d]
+    return jnp.roll(whole, shift, axis=d)
 
 
 def finish_heads(totals, weighted, lambdas, head_gain, kv_dev, group_size):
@@ -67,7 +78,7 @@
     own_tot = jnp.sum(parts_tot * factors, axis=0)
     own_acc = jnp.sum(parts_acc * factors[..., None], axis=0)
     own_out = finish_heads(own_tot, own_acc, lambdas, head_gain, kv_dev, group_size)
-    head_out = lax.all_gather(own_out, "kv", axis=0, tiled=True)
+    head_out = turned_line(own_out, "kv", 0)
     projected = jnp.dot(head_out, out_weight, preferred_element_type=jnp.float32)
     attn_out = lax.psum_scatter(
         projected.astype(jnp.bfloat16), "tp", scatter_dimension=1, tiled=True

time: 331 us -> 344 us (1.039)
  waiting for transfers between devices: 132 us -> 176 us
  blocking collectives: 123 us -> 92.4 us
    ppermute x0 -> x7, waiting for transfers between devices: none -> 43.9 us  [turned_line(): parts = [lax.ppermute(parts[0], axis, forward), *parts]]
    all_gather x1 -> x0, blocking collectives: 30.6 us -> none  [per_device(): head_out = lax.all_gather(own_out, 'kv', axis=0, tiled=True)]
    unnamed x18 -> x17, local copies, waits for them, and re-layouts: 24.3 us -> 24.3 us
  transfers between devices with their start and end apart: 7 -> 14, of which waited for: 7 -> 14; matrix products, arithmetic and copies ran while one was open for 8% -> 8% of each run, Pallas kernels for 0% -> 0%
where the time goes in v1:
time: 344 us; the launch traced here: 343 us
  waiting for transfers between devices  176 us (51%)
  blocking collectives  92.4 us (27%)
  local copies, waits for them, and re-layouts  26.1 us (8%)
  matrix products  18.6 us (5%)
  between operations  13.3 us (4%)
  starting transfers between devices  13.1 us (4%)
  other arithmetic  3.66 us (1%)
    psum x1, waiting for transfers between devices, per_device(): gate_sum, up_sum = lax.psum((gate_part, up_part), 'kv')  72.3 us
    ppermute x7, waiting for transfers between devices, turned_line(): parts = [lax.ppermute(parts[0], axis, forward), *parts]  43.9 us
    psum x1, blocking collectives, per_device(): squares = lax.psum(jnp.sum(own_cols * own_cols, axis=1), ('kv', 'tp'))  41 us
    psum x1, blocking collectives, per_device(): squares_two = lax.psum(jnp.sum(after_f * after_f, axis=1), ('kv', 'tp'))  39.3 us
    unnamed x6, waiting for transfers between devices  36.1 us
    unnamed x17, local copies, waits for them, and re-layouts  24.3 us
    psum x1, waiting for transfers between devices, per_device(): query_full = lax.psum(partial_value, 'kv')  9.04 us
    all_to_all x1, waiting for transfers between devices, per_device(): lax.all_to_all(weighted[None], 'kv', split_axis=2, concat_axis=0, tiled=T...  7.09 us
  transfers between devices with their start and end apart: 14, of which 14 were waited for; matrix products, arithmetic and copies ran while one was open for 8% of the time, Pallas kernels for 0%

profile of v1, /device:TPU:0, one launch (start us, length us, event | category | flops | bytes accessed | tf_op | source)
XLA Modules:
  0.0 342.7 jit_solution(5809537493440563807)
XLA Ops:
  6.5 6.5 %all_gather.6 = bf16[16,512]{1,0:T(8,128)(2,1)S(1)} all-gather(bf16[16,128]{1,0:T(8,128)(2,1)} %param.12), channel_id=1, replica_groups=mesh['kv'=8,'tp'=4] {'tp'}, dimensions={1}, use_global_device_ids=true | all-gather | bytes 20480 | tf_op jit(solution)/shard_map/all_gather | solution.py:46
  16.0 41.0 %psum.36 = f32[16]{0:T(128)S(1)} all-reduce(f32[16]{0:T(128)S(1)} %fusion.18), channel_id=1, replica_groups=mesh['kv'=8,'tp'=4] {'kv','tp'}, use_global_device_ids=true, to_apply=%region_2.0 | all-reduce | flops 16 | bytes 128 | tf_op jit(solution)/shard_map/psum | solution.py:51
  56.9 21.2 %copy.33 = bf16[16,1024,2,128]{1,3,2,0:T(8,128)(2,1)} copy(bf16[16,1024,2,128]{3,2,1,0:T(2,128)(2,1)} %param.15) | data formatting | bytes 16777216 | tf_op args[3]
  78.1 9.0 %all-reduce.4.cloned.1.call-done = f32[16,1024]{1,0:T(8,128)} async-done(((f32[16,1024]{1,0:T(8,128)}), f32[16,1024]{1,0:T(8,128)}) %all-reduce.4.cloned.1.call-update) | async-done | bytes 65552 | tf_op jit(solution)/shard_map/psum | solution.py:52
  88.2 4.7 %fusion.29 = (f32[2,16,2,4]{3,2,1,0:T(2,128)S(1)}, f32[2,16,2,4,1024]{4,3,2,1,0:T(4,128)S(1)}) fusion(bf16[16,1024,2,2,64]{1,4,3,2,0:T(8,128)(2,1)} %bitcast.53, bf16[16,2,4,2,64]{4,3,2,1,0:T(2,128)(2,1)S(1)} %reshape.35), kind=kOutput, calls=%fused_computation.47 | convolution fusion | flops 34078464 | bytes 9470976 | tf_op jit(solution)/shard_map/bkgcd,bpkcd->cbkgp/dot_general | solution.py:61
  94.1 4.5 %all-to-all-start.2 = ((f32[1,2,16,2,4]{4,3,1,0,2:T(2,128)}), f32[1,2,16,2,4]{4,3,1,0,2:T(2,128)S(1)}, u32[]{:S(2)}, u32[]{:S(2)}) async-start(f32[1,2,16,2,4]{4,3,1,0,2:T(2,128)} %copy.41), calls=%async_computation.2 | async-start | bytes 65536 | tf_op jit(solution)/shard_map/all_to_all | solution.py:73
  99.3 6.1 %all-to-all-done.2 = f32[1,2,16,2,4]{4,3,1,0,2:T(2,128)S(1)} async-done(((f32[1,2,16,2,4]{4,3,1,0,2:T(2,128)}), f32[1,2,16,2,4]{4,3,1,0,2:T(2,128)S(1)}, u32[]{:S(2)}, u32[]{:S(2)}) %all-to-all-start.2) | async-done | bytes 1056 | tf_op jit(solution)/shard_map/all_to_all | solution.py:73
  105.3 3.3 all-to-all-start.1
  108.7 5.5 %fusion.7 = f32[1,2,16,2,4,128]{5,4,1,3,0,2:T(4,128)} fusion(bf16[16,1024,2,128,1]{3,2,1,0,4:T(2,128)(2,1)} %bitcast.66, bf16[2,16,2,4,1024]{4,3,2,1,0:T(4,128)(2,1)S(1)} %get-tuple-element.10), kind=kOutput, calls=%fused_computation.5 | convolution fusion | flops 67108864 | bytes 9043968 | tf_op jit(solution)/shard_map/cbkgp,bpkv->cbkgv/dot_general | solution.py:68
  115.3 4.8 %all-to-all-start = ((f32[1,2,16,2,4,128]{5,4,1,3,0,2:T(4,128)}), f32[1,2,16,2,4,128]{5,4,1,3,0,2:T(4,128)S(1)}, u32[]{:S(2)}, u32[]{:S(2)}) async-start(f32[1,2,16,2,4,128]{5,4,1,3,0,2:T(4,128)} %fusion.7), calls=%async_computation | async-start | bytes 262144 | tf_op jit(solution)/shard_map/all_to_all | solution.py:74
  120.4 7.1 %all-to-all-done = f32[1,2,16,2,4,128]{5,4,1,3,0,2:T(4,128)S(1)} async-done(((f32[1,2,16,2,4,128]{5,4,1,3,0,2:T(4,128)}), f32[1,2,16,2,4,128]{5,4,1,3,0,2:T(4,128)S(1)}, u32[]{:S(2)}, u32[]{:S(2)}) %all-to-all-start) | async-done | bytes 131104 | tf_op jit(solution)/shard_map/all_to_all | solution.py:74
  128.4 6.1 %collective-permute-done = bf16[2,1024]{1,0:T(2,128)(2,1)S(1)} collective-permute-done((bf16[2,1024]{1,0:T(2,128)(2,1)S(1)}, bf16[2,1024]{1,0:T(2,128)(2,1)S(1)}, u32[]{:S(2)}, u32[]{:S(2)}) %collective-permute-start) | collective-permute-done | bytes 4128 | tf_op jit(solution)/shard_map/ppermute | solution.py:16
  134.5 6.3 %collective-permute-done.1 = bf16[2,1024]{1,0:T(2,128)(2,1)S(1)} collective-permute-done((bf16[2,1024]{1,0:T(2,128)(2,1)S(1)}, bf16[2,1024]{1,0:T(2,128)(2,1)S(1)}, u32[]{:S(2)}, u32[]{:S(2)}) %collective-permute-start.1) | collective-permute-done | bytes 4128 | tf_op jit(solution)/shard_map/ppermute | solution.py:16
  140.8 6.3 %collective-permute-done.2 = bf16[2,1024]{1,0:T(2,128)(2,1)S(1)} collective-permute-done((bf16[2,1024]{1,0:T(2,128)(2,1)S(1)}, bf16[2,1024]{1,0:T(2,128)(2,1)S(1)}, u32[]{:S(2)}, u32[]{:S(2)}) %collective-permute-start.2) | collective-permute-done | bytes 4128 | tf_op jit(solution)/shard_map/ppermute | solution.py:16
  147.1 6.3 %collective-permute-done.3 = bf16[2,1024]{1,0:T(2,128)(2,1)S(1)} collective-permute-done((bf16[2,1024]{1,0:T(2,128)(2,1)S(1)}, bf16[2,1024]{1,0:T(2,128)(2,1)S(1)}, u32[]{:S(2)}, u32[]{:S(2)}) %collective-permute-start.3) | collective-permute-done | bytes 4128 | tf_op jit(solution)/shard_map/ppermute | solution.py:16
  153.4 6.3 %collective-permute-done.4 = bf16[2,1024]{1,0:T(2,128)(2,1)S(1)} collective-permute-done((bf16[2,1024]{1,0:T(2,128)(2,1)S(1)}, bf16[2,1024]{1,0:T(2,128)(2,1)S(1)}, u32[]{:S(2)}, u32[]{:S(2)}) %collective-permute-start.4) | collective-permute-done | bytes 4128 | tf_op jit(solution)/shard_map/ppermute | solution.py:16
  159.7 6.3 %collective-permute-done.5 = bf16[2,1024]{1,0:T(2,128)(2,1)S(1)} collective-permute-done((bf16[2,1024]{1,0:T(2,128)(2,1)S(1)}, bf16[2,1024]{1,0:T(2,128)(2,1)S(1)}, u32[]{:S(2)}, u32[]{:S(2)}) %collective-permute-start.5) | collective-permute-done | bytes 4128 | tf_op jit(solution)/shard_map/ppermute | solution.py:16
  166.0 6.3 %collective-permute-done.6 = bf16[2,1024]{1,0:T(2,128)(2,1)S(1)} collective-permute-done((bf16[2,1024]{1,0:T(2,128)(2,1)S(1)}, bf16[2,1024]{1,0:T(2,128)(2,1)S(1)}, u32[]{:S(2)}, u32[]{:S(2)}) %collective-permute-start.6) | collective-permute-done | bytes 4128 | tf_op jit(solution)/shard_map/ppermute | solution.py:16
  174.8 17.0 %reduce-scatter.7.cloned.1.call-done = bf16[128,16]{1,0:T(8,128)(2,1)} async-done(((bf16[512,16]{1,0:T(8,128)(2,1)}), bf16[128,16]{1,0:T(8,128)(2,1)}) %reduce-scatter.7.cloned.1.call-update) | async-done | bytes 4112
  192.7 39.3 %psum.37 = f32[16]{0:T(128)S(1)} all-reduce(f32[16]{0:T(128)S(1)} %fusion.20), channel_id=1, replica_groups=mesh['kv'=8,'tp'=4] {'kv','tp'}, use_global_device_ids=true, to_apply=%region_11.12 | all-reduce | flops 16 | bytes 128 | tf_op jit(solution)/shard_map/psum | solution.py:88
  232.1 5.6 %all_gather.7 = bf16[16,512]{1,0:T(8,128)(2,1)S(1)} all-gather(bf16[16,128]{1,0:T(8,128)(2,1)S(1)} %fusion.22), channel_id=1, replica_groups=mesh['kv'=8,'tp'=4] {'tp'}, dimensions={1}, use_global_device_ids=true | all-gather | bytes 20480 | tf_op jit(solution)/shard_map/all_gather | solution.py:92
  240.1 72.3 %all-reduce.6.cloned.1.call-done = (f32[16,2816]{1,0:T(8,128)}, f32[16,2816]{1,0:T(8,128)}) async-done(((f32[16,2816]{1,0:T(8,128)}, f32[16,2816]{1,0:T(8,128)}), (f32[16,2816]{1,0:T(8,128)}, f32[16,2816]{1,0:T(8,128)})) %all-reduce.6.cloned.1.call-update) | async-done | bytes 360464 | tf_op jit(solution)/shard_map/psum | solution.py:95
  312.4 2.5 convolution_convert_fusion
  315.7 19.1 %reduce-scatter.9.cloned.1.call-done = bf16[128,16]{1,0:T(8,128)(2,1)} async-done(((bf16[512,16]{1,0:T(8,128)(2,1)}), bf16[128,16]{1,0:T(8,128)(2,1)}) %reduce-scatter.9.cloned.1.call-update) | async-done | bytes 4112
  (65 shorter events, 16.1 us)
Async XLA Ops:
  6.5 231.1 %copy-start = (bf16[512,2816]{1,0:T(8,128)(2,1)S(1)}, bf16[512,2816]{1,0:T(8,128)(2,1)}, u32[]{:S(2)}) copy-start(bf16[512,2816]{1,0:T(8,128)(2,1)} %param.21) | copy-start | bytes 8650756
  6.5 80.6 %all-reduce.4.cloned.1.call-start = ((), (), s32[]{:S(2)}) async-start(), calls=%async_computation.5 | async-start | bytes 131072 | tf_op jit(solution)/shard_map/psum | solution.py:52
  94.1 11.2 %all-to-all-start.2 = ((f32[1,2,16,2,4]{4,3,1,0,2:T(2,128)}), f32[1,2,16,2,4]{4,3,1,0,2:T(2,128)S(1)}, u32[]{:S(2)}, u32[]{:S(2)}) async-start(f32[1,2,16,2,4]{4,3,1,0,2:T(2,128)} %copy.41), calls=%async_computation.2 | async-start | bytes 65536 | tf_op jit(solution)/shard_map/all_to_all | solution.py:73
  105.3 10.0 %all-to-all-start.1 = ((f32[1,2,16,2,4]{4,3,1,0,2:T(2,128)}), f32[1,2,16,2,4]{4,3,1,0,2:T(2,128)S(1)}, u32[]{:S(2)}, u32[]{:S(2)}) async-start(f32[1,2,16,2,4]{4,3,1,0,2:T(2,128)} %copy.39), calls=%async_computation.1 | async-start | bytes 65536 | tf_op jit(solution)/shard_map/all_to_all | solution.py:72
  108.7 11.5 %copy-start.5 = (f32[8]{0:T(128)S(1)}, f32[8]{0:T(128)}, u32[]{:S(2)}) copy-start(f32[8]{0:T(128)} %param.17) | copy-start | bytes 100
  108.7 19.4 %copy-start.3 = (f32[128]{0:T(128)S(1)}, f32[128]{0:T(128)}, u32[]{:S(2)}) copy-start(f32[128]{0:T(128)} %param.18) | copy-start | bytes 1540
  108.7 83.9 %copy-start.2 = (bf16[16,128]{1,0:T(8,128)(2,1)S(1)}, bf16[16,128]{1,0:T(8,128)(2,1)}, u32[]{:S(2)}) copy-start(bf16[16,128]{1,0:T(8,128)(2,1)} %param.12) | copy-start | bytes 12292
  108.7 123.3 %copy-start.4 = (f32[128]{0:T(128)S(1)}, f32[128]{0:T(128)}, u32[]{:S(2)}) copy-start(f32[128]{0:T(128)} %param.20) | copy-start | bytes 1540
  115.3 12.2 %all-to-all-start = ((f32[1,2,16,2,4,128]{5,4,1,3,0,2:T(4,128)}), f32[1,2,16,2,4,128]{5,4,1,3,0,2:T(4,128)S(1)}, u32[]{:S(2)}, u32[]{:S(2)}) async-start(f32[1,2,16,2,4,128]{5,4,1,3,0,2:T(4,128)} %fusion.7), calls=%async_computation | async-start | bytes 262144 | tf_op jit(solution)/shard_map/all_to_all | solution.py:74
  120.1 71.6 %reduce-scatter.7.cloned.1.call-start = ((), (), s32[]{:S(2)}) async-start(), calls=%async_computation.6 | async-start | bytes 163840
  128.1 6.4 %collective-permute-start = (bf16[2,1024]{1,0:T(2,128)(2,1)S(1)}, bf16[2,1024]{1,0:T(2,128)(2,1)S(1)}, u32[]{:S(2)}, u32[]{:S(2)}) collective-permute-start(bf16[2,1024]{1,0:T(2,128)(2,1)S(1)} %multiply_convert_fusion.5), channel_id=1, source_target_pairs={{0,4},{4,8},{8,12},{12,16},{16,20},{20,24},{24,28},{28,0},{1,5},{5... | collective-permute-start | bytes 12296 | tf_op jit(solution)/shard_map/ppermute | solution.py:16
  134.5 6.3 %collective-permute-start.1 = (bf16[2,1024]{1,0:T(2,128)(2,1)S(1)}, bf16[2,1024]{1,0:T(2,128)(2,1)S(1)}, u32[]{:S(2)}, u32[]{:S(2)}) collective-permute-start(bf16[2,1024]{1,0:T(2,128)(2,1)S(1)} %collective-permute-done), channel_id=1, source_target_pairs={{0,4},{4,8},{8,12},{12,16},{16,20},{20,24},{24,28},{28,0},{1,5},{5... | collective-permute-start | bytes 12296 | tf_op jit(solution)/shard_map/ppermute | solution.py:16
  140.8 6.3 %collective-permute-start.2 = (bf16[2,1024]{1,0:T(2,128)(2,1)S(1)}, bf16[2,1024]{1,0:T(2,128)(2,1)S(1)}, u32[]{:S(2)}, u32[]{:S(2)}) collective-permute-start(bf16[2,1024]{1,0:T(2,128)(2,1)S(1)} %collective-permute-done.1), channel_id=1, source_target_pairs={{0,4},{4,8},{8,12},{12,16},{16,20},{20,24},{24,28},{28,0},{1,5},{5... | collective-permute-start | bytes 12296 | tf_op jit(solution)/shard_map/ppermute | solution.py:16
  147.1 6.3 %collective-permute-start.3 = (bf16[2,1024]{1,0:T(2,128)(2,1)S(1)}, bf16[2,1024]{1,0:T(2,128)(2,1)S(1)}, u32[]{:S(2)}, u32[]{:S(2)}) collective-permute-start(bf16[2,1024]{1,0:T(2,128)(2,1)S(1)} %collective-permute-done.2), channel_id=1, source_target_pairs={{0,4},{4,8},{8,12},{12,16},{16,20},{20,24},{24,28},{28,0},{1,5},{5... | collective-permute-start | bytes 12296 | tf_op jit(solution)/shard_map/ppermute | solution.py:16
  153.4 6.3 %collective-permute-start.4 = (bf16[2,1024]{1,0:T(2,128)(2,1)S(1)}, bf16[2,1024]{1,0:T(2,128)(2,1)S(1)}, u32[]{:S(2)}, u32[]{:S(2)}) collective-permute-start(bf16[2,1024]{1,0:T(2,128)(2,1)S(1)} %collective-permute-done.3), channel_id=1, source_target_pairs={{0,4},{4,8},{8,12},{12,16},{16,20},{20,24},{24,28},{28,0},{1,5},{5... | collective-permute-start | bytes 12296 | tf_op jit(solution)/shard_map/ppermute | solution.py:16
  159.7 6.3 %collective-permute-start.5 = (bf16[2,1024]{1,0:T(2,128)(2,1)S(1)}, bf16[2,1024]{1,0:T(2,128)(2,1)S(1)}, u32[]{:S(2)}, u32[]{:S(2)}) collective-permute-start(bf16[2,1024]{1,0:T(2,128)(2,1)S(1)} %collective-permute-done.4), channel_id=1, source_target_pairs={{0,4},{4,8},{8,12},{12,16},{16,20},{20,24},{24,28},{28,0},{1,5},{5... | collective-permute-start | bytes 12296 | tf_op jit(solution)/shard_map/ppermute | solution.py:16
  166.0 6.3 %collective-permute-start.6 = (bf16[2,1024]{1,0:T(2,128)(2,1)S(1)}, bf16[2,1024]{1,0:T(2,128)(2,1)S(1)}, u32[]{:S(2)}, u32[]{:S(2)}) collective-permute-start(bf16[2,1024]{1,0:T(2,128)(2,1)S(1)} %collective-permute-done.5), channel_id=1, source_target_pairs={{0,4},{4,8},{8,12},{12,16},{16,20},{20,24},{24,28},{28,0},{1,5},{5... | collective-permute-start | bytes 12296 | tf_op jit(solution)/shard_map/ppermute | solution.py:16
  174.7 137.7 %all-reduce.6.cloned.1.call-start = ((), (), s32[]{:S(2)}) async-start(), calls=%async_computation.8 | async-start | bytes 720896 | tf_op jit(solution)/shard_map/psum | solution.py:95
  232.0 6.8 %copy-start.1 = (bf16[512,2816]{1,0:T(8,128)(2,1)S(1)}, bf16[512,2816]{1,0:T(8,128)(2,1)}, u32[]{:S(2)}) copy-start(bf16[512,2816]{1,0:T(8,128)(2,1)} %param.22) | copy-start | bytes 8650756
  240.0 94.8 %reduce-scatter.9.cloned.1.call-start = ((), (), s32[]{:S(2)}) async-start(), calls=%async_computation.7 | async-start | bytes 163840
Sparse Core Ops, SparseCore 0:
  16.1 71.0 all-reduce.3
  174.8 16.8 reduce-scatter.6
  240.1 72.2 all-reduce.5
  315.8 18.9 reduce-scatter.8
